TPU v7x, 32 devices: a whole 2x2x4 slice. The times are simulated.
32 devices in a mesh: gr: 2 (over y), fs: 4 (over z), tp: 4 (over x, core).
Axes of the slice: x: 2, y: 2, z: 4, core: 2. Of those that a mesh axis runs over, the one named last changes fastest.
Arguments:
- tokens: bfloat16 [4096, 2048], P(('gr', 'tp'), 'fs'), may hold values from -6 to 6
- routes: int32 [4096, 2], P(('gr', 'tp')), may hold values from 0 to 7, all different within a row; in each aligned block of 512 rows (0 to 511, 512 to 1023, ...) at most 192 rows name the same one
- route_weight: float32 [4096, 2], P(('gr', 'tp')), may hold values from 0.25 to 1
- norm_gain: float32 [2048], P(('gr', 'fs')), may hold values from 0.1 to 1.9
- gate_master: float32 [8, 2048, 2816], P(None, ('gr', 'fs'), 'tp'), may hold values from -0.125 to 0.125
- up_master: float32 [8, 2048, 2816], P(None, ('gr', 'fs'), 'tp'), may hold values from -0.125 to 0.125
- down_master: float32 [8, 2048, 2816], P(None, ('gr', 'fs'), 'tp'), may hold values from -0.109375 to 0.109375
Outputs:
- mixed_output: bfloat16 [4096, 2048], P(('gr', 'tp'), 'fs')
- gate_serving: bfloat16 [8, 2048, 2816], P('tp', None, 'fs')
- up_serving: bfloat16 [8, 2048, 2816], P('tp', None, 'fs')
- down_serving: bfloat16 [8, 2048, 2816], P('tp', None, 'fs')
Inputs may be any that keep to these rules, and one draw needn't show every extreme that they name: `routes`: each row names two different experts. Within the rows of one block of 512 tokens (one index of gr+tp) no expert is named by more than 192 rows, and in some blocks one expert is named by exactly 192.
All inputs are finite; a program needn't handle non-finite values.
Results may differ from a plain program's by a relative error of at most 0.0082.
Values may be sent and summed in bfloat16 or wider, within the bound.
A program may use at most 128 MiB of HBM per device.

v0:
```python
import jax
import jax.numpy as jnp
from jax import lax
from jax.sharding import PartitionSpec as P

norm_eps = 1e-06


def slot_table(routes, experts, capacity):
    flat_routes = routes.reshape(-1)
    onehot = (flat_routes[:, None] == jnp.arange(experts, dtype=jnp.int32)[None, :]).astype(
        jnp.int32
    )
    running = jnp.cumsum(onehot, axis=0)
    slot_index = jnp.sum(onehot * (running - 1), axis=1)
    return flat_routes * capacity + slot_index


def spread(gate_w, up_w, down_w):
    gate_e, up_e, down_e = (
        lax.all_to_all(gate_w, "tp", split_axis=0, concat_axis=2, tiled=True),
        lax.all_to_all(up_w, "tp", split_axis=0, concat_axis=2, tiled=True),
        lax.all_to_all(down_w, "tp", split_axis=0, concat_axis=2, tiled=True),
    )
    return (
        lax.all_to_all(gate_e, "fs", split_axis=2, concat_axis=1, tiled=True),
        lax.all_to_all(up_e, "fs", split_axis=2, concat_axis=1, tiled=True),
        lax.all_to_all(down_e, "fs", split_axis=2, concat_axis=1, tiled=True),
    )


def local(tokens, routes, route_weight, norm_gain, gate_master, up_master, down_master):
    experts = gate_master.shape[0]
    tp_count = lax.axis_size("tp")
    fs_count = lax.axis_size("fs")
    local_experts = experts // tp_count
    token_rows = tokens.shape[0]
    model_width = tokens.shape[1] * fs_count
    capacity = 3 * token_rows // experts
    scaled_gain = norm_gain[None, :, None]
    gate_w = (gate_master * scaled_gain).astype(jnp.bfloat16)
    up_w = (up_master * scaled_gain).astype(jnp.bfloat16)
    down_w = down_master.astype(jnp.bfloat16)
    gate_w, up_w, down_w = spread(gate_w, up_w, down_w)
    gate_w, up_w, down_w = (
        lax.all_gather(gate_w, "gr", axis=1, tiled=True),
        lax.all_gather(up_w, "gr", axis=1, tiled=True),
        lax.all_gather(down_w, "gr", axis=1, tiled=True),
    )
    as_float = tokens.astype(jnp.float32)
    square_total = lax.psum(jnp.sum(as_float * as_float, axis=1), "fs")
    normed = (as_float * lax.rsqrt(square_total / model_width + norm_eps)[:, None]).astype(
        jnp.bfloat16
    )
    placing = slot_table(routes, experts, capacity)
    slot_rows = jnp.arange(experts * capacity, dtype=jnp.int32)
    picked = (slot_rows[:, None] == placing[None, :]).reshape(experts * capacity, token_rows, 2)
    route_table = jnp.sum(picked.astype(jnp.float32), axis=2).astype(jnp.bfloat16)
    outgoing = jnp.dot(route_table, normed, preferred_element_type=jnp.float32).astype(jnp.bfloat16)
    outgoing = outgoing.reshape(tp_count, local_experts, capacity, tokens.shape[1])
    shard_piece = lax.all_gather(
        lax.all_to_all(outgoing, "tp", split_axis=0, concat_axis=0, tiled=True),
        "fs",
        axis=3,
        tiled=True,
    )
    gate_acc = jnp.einsum("sjcd,jdf->sjcf", shard_piece, gate_w, preferred_element_type=jnp.float32)
    up_acc = jnp.einsum("sjcd,jdf->sjcf", shard_piece, up_w, preferred_element_type=jnp.float32)
    gate_acc, up_acc = (gate_acc, up_acc)
    hidden = (jax.nn.silu(gate_acc) * up_acc).astype(jnp.bfloat16)
    partial_value = jnp.einsum("sjcf,jdf->sjcd", hidden, down_w, preferred_element_type=jnp.float32)
    summed = lax.psum_scatter(partial_value, "fs", scatter_dimension=3, tiled=True)
    produced = lax.all_to_all(summed, "tp", split_axis=0, concat_axis=0, tiled=True)
    produced = produced.reshape(experts * capacity, produced.shape[3])
    pair_slots = placing.reshape(token_rows, 2)
    first_rows = jnp.take(produced, pair_slots[:, 0], axis=0)
    second_rows = jnp.take(produced, pair_slots[:, 1], axis=0)
    mixed_out = first_rows * route_weight[:, 0:1] + second_rows * route_weight[:, 1:2]
    return (mixed_out.astype(jnp.bfloat16), gate_w, up_w, down_w)


def solution(mesh):
    placed = (
        P(("gr", "tp"), "fs"),
        P(("gr", "tp"), None),
        P(("gr", "tp"), None),
        P(("gr", "fs")),
        P(None, ("gr", "fs"), "tp"),
        P(None, ("gr", "fs"), "tp"),
        P(None, ("gr", "fs"), "tp"),
    )
    return jax.shard_map(
        local,
        mesh=mesh,
        in_specs=placed,
        out_specs=(
            P(("gr", "tp"), "fs"),
            P("tp", None, "fs"),
            P("tp", None, "fs"),
            P("tp", None, "fs"),
        ),
        check_vma=False,
    )
```

profile of v0, /device:TPU:0, one launch (start us, length us, event | category | flops | bytes accessed | tf_op | source)
XLA Modules:
  0.0 855.1 jit_solution(9857111797284173480)
XLA Ops:
  8.4 2.3 reduce-window.6
  15.0 13.5 %psum.7 = f32[512]{0:T(512)S(1)} all-reduce(f32[512]{0:T(512)S(1)} %fusion.18), channel_id=1, replica_groups=mesh['gr'=2,'fs'=4,'tp'=4] {'fs'}, use_global_device_ids=true, to_apply=%region_5.6 | all-reduce | flops 512 | bytes 4096 | tf_op jit(solution)/shard_map/psum | solution.py:51
  30.6 22.6 %all_to_all.118 = bf16[4,2,192,512]{3,2,1,0:T(8,128)(2,1)S(1)} all-to-all(bf16[4,2,192,512]{3,2,1,0:T(8,128)(2,1)S(1)} %bitcast.113), channel_id=1, replica_groups=mesh['gr'=2,'fs'=4,'tp'=4] {'tp'}, dimensions={0} | all-to-all | bytes 3145728 | tf_op jit(solution)/shard_map/all_to_all | solution.py:62
  54.5 7.2 multiply_convert_fusion.1
  61.7 36.6 %all_to_all.119 = bf16[8,256,704]{1,2,0:T(8,128)(2,1)S(1)} all-to-all(bf16[8,256,704]{1,2,0:T(8,128)(2,1)S(1)} %get-tuple-element.10), channel_id=1, replica_groups=mesh['gr'=2,'fs'=4,'tp'=4] {'tp'}, dimensions={0} | all-to-all | bytes 5767168 | tf_op jit(solution)/shard_map/all_to_all | solution.py:22
  98.4 17.6 %copy.79 = bf16[2,256,2816]{1,0,2:T(2,128)(2,1)S(1)} copy(bf16[2,256,2816]{1,2,0:T(8,128)(2,1)S(1)} %bitcast.103) | data formatting | bytes 5767168 | tf_op jit(solution)/shard_map/all_to_all | solution.py:22
  116.0 112.6 %all_to_all.120 = bf16[2,256,2816]{1,0,2:T(2,128)(2,1)} all-to-all(bf16[2,256,2816]{1,0,2:T(2,128)(2,1)S(1)} %copy.79), channel_id=1, replica_groups=mesh['gr'=2,'fs'=4,'tp'=4] {'fs'}, dimensions={2} | all-to-all | bytes 5767168 | tf_op jit(solution)/shard_map/all_to_all | solution.py:27
  228.6 3.7 all-to-all-start
  232.4 2.2 copy.80
  236.6 29.8 %all-to-all-done = bf16[8,256,704]{1,2,0:T(8,128)(2,1)S(1)} async-done(((bf16[8,256,704]{1,2,0:T(8,128)(2,1)}), bf16[8,256,704]{1,2,0:T(8,128)(2,1)S(1)}, u32[]{:S(2)}, u32[]{:S(2)}) %all-to-all-start) | async-done | bytes 2883616 | tf_op jit(solution)/shard_map/all_to_all | solution.py:21
  266.6 19.0 %copy.74 = bf16[2,256,2816]{1,0,2:T(2,128)(2,1)} copy(bf16[2,256,2816]{1,2,0:T(8,128)(2,1)S(1)} %bitcast.105) | data formatting | bytes 5767168 | tf_op jit(solution)/shard_map/all_to_all | solution.py:21
  285.6 3.7 all-to-all-start.1
  289.2 4.5 convert_element_type.44
  293.8 60.6 %all-to-all-done.1 = bf16[2,256,2816]{1,0,2:T(2,128)(2,1)S(1)} async-done(((bf16[2,256,2816]{1,0,2:T(2,128)(2,1)}), bf16[2,256,2816]{1,0,2:T(2,128)(2,1)S(1)}, u32[]{:S(2)}, u32[]{:S(2)}) %all-to-all-start.1) | async-done | bytes 2883616 | tf_op jit(solution)/shard_map/all_to_all | solution.py:26
  355.9 3.7 all-to-all-start.5
  359.7 2.2 copy.75
  364.1 29.6 %all-to-all-done.5 = bf16[8,256,704]{1,2,0:T(8,128)(2,1)S(1)} async-done(((bf16[8,256,704]{1,2,0:T(8,128)(2,1)}), bf16[8,256,704]{1,2,0:T(8,128)(2,1)S(1)}, u32[]{:S(2)}, u32[]{:S(2)}) %all-to-all-start.5) | async-done | bytes 2883616 | tf_op jit(solution)/shard_map/all_to_all | solution.py:23
  393.9 17.6 %copy.83 = bf16[2,256,2816]{1,0,2:T(2,128)(2,1)S(1)} copy(bf16[2,256,2816]{1,2,0:T(8,128)(2,1)S(1)} %bitcast.107) | data formatting | bytes 5767168 | tf_op jit(solution)/shard_map/all_to_all | solution.py:23
  411.4 67.6 %all_to_all.121 = bf16[2,256,2816]{1,0,2:T(2,128)(2,1)S(1)} all-to-all(bf16[2,256,2816]{1,0,2:T(2,128)(2,1)S(1)} %copy.83), channel_id=1, replica_groups=mesh['gr'=2,'fs'=4,'tp'=4] {'fs'}, dimensions={2} | all-to-all | bytes 5767168 | tf_op jit(solution)/shard_map/all_to_all | solution.py:28
  481.6 10.3 %fusion.2 = f32[2,704,4,192]{1,3,2,0:T(8,128)} fusion(bf16[4,2,192,2048]{3,2,0,1:T(8,128)(2,1)} %all-gather.7.cloned.1.call-done, bf16[2,2048,704]{1,2,0:T(8,128)(2,1)} %all-gather.9.cloned.1.call-done), kind=kOutput, calls=%fused_computation.6 | convolution fusion | flops 4429185024 | bytes 16384000 | tf_op jit(solution)/shard_map/sjcd,jdf->sjcf/dot_general | solution.py:68
  491.8 62.6 %all-gather.11.cloned.1.call-done = bf16[2,2048,704]{1,2,0:T(8,128)(2,1)} async-done(((bf16[2,1024,704]{1,2,0:T(8,128)(2,1)}), bf16[2,2048,704]{1,2,0:T(8,128)(2,1)}) %all-gather.11.cloned.1.call-update) | async-done | bytes 5767184 | tf_op jit(solution)/shard_map/all_gather | solution.py:48
  554.5 18.6 %fusion.6 = f32[4,2,192,2048]{3,2,0,1:T(8,128)} fusion(bf16[2,2048,704]{1,2,0:T(8,128)(2,1)} %all-gather.11.cloned.1.call-done, f32[2,704,4,192]{1,3,2,0:T(8,128)} %fusion.2, bf16[4,2,192,2048]{3,2,0,1:T(8,128)(2,1)} %all-gather.7.cloned.1.call-done, bf16[2,2048,704]{1,2,0:T(8,128)(2,1)} %all-gather.5.cloned.1.call-done), kind=kOutput, calls=%fused_computation.12 | convolution fusion | flops 8864858112 | bytes 34734080 | tf_op jit(solution)/shard_map/sjcf,jdf->sjcd/dot_general | solution.py:71
  573.1 212.0 %reduce-scatter.2.cloned.1.call-done = f32[4,2,192,512]{3,2,0,1:T(8,128)} async-done(((f32[4,2,192,2048]{3,2,0,1:T(8,128)}), f32[4,2,192,512]{3,2,0,1:T(8,128)}) %reduce-scatter.2.cloned.1.call-update) | async-done | bytes 3145744 | tf_op jit(solution)/shard_map/reduce_scatter | solution.py:72
  785.1 3.9 copy.86
  789.0 3.8 all-to-all-start.7
  792.9 36.8 %all-to-all-done.7 = f32[4,2,192,512]{3,2,1,0:T(8,128)S(1)} async-done(((f32[4,2,192,512]{3,2,1,0:T(8,128)}), f32[4,2,192,512]{3,2,1,0:T(8,128)S(1)}, u32[]{:S(2)}, u32[]{:S(2)}) %all-to-all-start.7) | async-done | bytes 3145760 | tf_op jit(solution)/shard_map/all_to_all | solution.py:73
  829.7 2.3 gather_fusion
  832.0 2.3 gather_fusion.1
  834.3 2.8 fusion.21
  837.2 6.3 copy.98
  843.5 2.5 copy.99
  846.0 2.5 copy.100
  (59 shorter events, 17.9 us)
Async XLA Ops:
  7.2 474.4 %all-gather.7.cloned.1.call-start = ((), (), s32[]{:S(2)}) async-start(), calls=%async_computation.10 | async-start | bytes 7864320 | tf_op jit(solution)/shard_map/all_gather | solution.py:61
  30.6 23.9 %copy-start.2 = (f32[256]{0:T(256)S(1)}, f32[256]{0:T(256)}, u32[]{:S(2)}) copy-start(f32[256]{0:T(256)} %param.12) | copy-start | bytes 3076
  228.6 37.7 %all-to-all-start = ((bf16[8,256,704]{1,2,0:T(8,128)(2,1)}), bf16[8,256,704]{1,2,0:T(8,128)(2,1)S(1)}, u32[]{:S(2)}, u32[]{:S(2)}) async-start(bf16[8,256,704]{1,2,0:T(8,128)(2,1)} %get-tuple-element.9), calls=%async_computation | async-start | bytes 5767168 | tf_op jit(solution)/shard_map/all_to_all | solution.py:21
  232.3 249.2 %all-gather.9.cloned.1.call-start = ((), (), s32[]{:S(2)}) async-start(), calls=%async_computation.11 | async-start | bytes 8650752 | tf_op jit(solution)/shard_map/all_gather | solution.py:47
  285.6 68.8 %all-to-all-start.1 = ((bf16[2,256,2816]{1,0,2:T(2,128)(2,1)}), bf16[2,256,2816]{1,0,2:T(2,128)(2,1)S(1)}, u32[]{:S(2)}, u32[]{:S(2)}) async-start(bf16[2,256,2816]{1,0,2:T(2,128)(2,1)} %copy.74), calls=%async_computation.1 | async-start | bytes 5767168 | tf_op jit(solution)/shard_map/all_to_all | solution.py:26
  354.4 1.6 copy-start
  355.9 37.7 %all-to-all-start.5 = ((bf16[8,256,704]{1,2,0:T(8,128)(2,1)}), bf16[8,256,704]{1,2,0:T(8,128)(2,1)S(1)}, u32[]{:S(2)}, u32[]{:S(2)}) async-start(bf16[8,256,704]{1,2,0:T(8,128)(2,1)} %convert_element_type.44), calls=%async_computation.5 | async-start | bytes 5767168 | tf_op jit(solution)/shard_map/all_to_all | solution.py:23
  359.6 132.2 %all-gather.5.cloned.1.call-start = ((), (), s32[]{:S(2)}) async-start(), calls=%async_computation.9 | async-start | bytes 8650752 | tf_op jit(solution)/shard_map/all_gather | solution.py:46
  363.9 190.6 %all-gather.11.cloned.1.call-start = ((), (), s32[]{:S(2)}) async-start(), calls=%async_computation.12 | async-start | bytes 8650752 | tf_op jit(solution)/shard_map/all_gather | solution.py:48
  481.5 303.7 %reduce-scatter.2.cloned.1.call-start = ((), (), s32[]{:S(2)}) async-start(), calls=%async_computation.13 | async-start | bytes 15728640 | tf_op jit(solution)/shard_map/reduce_scatter | solution.py:72
  789.0 3.9 copy-start.1
  789.0 40.7 %all-to-all-start.7 = ((f32[4,2,192,512]{3,2,1,0:T(8,128)}), f32[4,2,192,512]{3,2,1,0:T(8,128)S(1)}, u32[]{:S(2)}, u32[]{:S(2)}) async-start(f32[4,2,192,512]{3,2,1,0:T(8,128)} %copy.86), calls=%async_computation.8 | async-start | bytes 6291456 | tf_op jit(solution)/shard_map/all_to_all | solution.py:73
  834.3 9.1 %slice-start = ((s8[5767168]{0:T(1024)(128)(4,1)}), s8[4194304]{0:T(1024)(128)(4,1)S(1)}, s32[]{:S(2)}) async-start(s8[5767168]{0:T(1024)(128)(4,1)} %bitcast.109), calls=%async_computation.14 | async-start | bytes 8388608
  837.2 6.3 slice-start.1
  837.2 8.9 %slice-start.2 = ((s8[5767168]{0:T(1024)(128)(4,1)}), s8[4194304]{0:T(1024)(128)(4,1)S(1)}, s32[]{:S(2)}) async-start(s8[5767168]{0:T(1024)(128)(4,1)} %bitcast.111), calls=%async_computation.16 | async-start | bytes 8388608
  843.5 2.5 slice-start.3
Sparse Core Ops, SparseCore 0:
  54.6 165.7 all-gather.6
  236.7 73.0 all-gather.8
  364.0 73.9 all-gather.4
  481.6 72.8 all-gather.10
  573.2 211.8 reduce-scatter.1
where the time goes:
time: 856 us; the launch traced here: 855 us
  waiting for transfers between devices  431 us (50%)
  blocking collectives  253 us (30%)
  local copies, waits for them, and re-layouts  89.9 us (11%)
  matrix products  31 us (4%)
  other arithmetic  20.6 us (2%)
  starting transfers between devices  15.2 us (2%)
  between operations  14 us (2%)
    reduce_scatter x1, waiting for transfers between devices, local(): lax.psum_scatter(partial_value, 'fs', scatter_dimension=3, tiled=True)  212 us
    all_to_all x1, blocking collectives, spread(): lax.all_to_all(up_e, 'fs', split_axis=2, concat_axis=1, tiled=True)  113 us
    all_to_all x1, blocking collectives, spread(): lax.all_to_all(down_e, 'fs', split_axis=2, concat_axis=1, tiled=True)  67.6 us
    all_gather x1, waiting for transfers between devices, local(): lax.all_gather(down_w, 'gr', axis=1, tiled=True)  62.6 us
    all_to_all x1, waiting for transfers between devices, spread(): lax.all_to_all(gate_e, 'fs', split_axis=2, concat_axis=1, tiled=True)  60.6 us
    all_to_all x1, waiting for transfers between devices, local(): lax.all_to_all(summed, 'tp', split_axis=0, concat_axis=0, tiled=True)  36.8 us
    all_to_all x1, blocking collectives, spread(): lax.all_to_all(up_w, 'tp', split_axis=0, concat_axis=2, tiled=True)  36.6 us
    all_to_all x1, waiting for transfers between devices, spread(): lax.all_to_all(gate_w, 'tp', split_axis=0, concat_axis=2, tiled=True)  29.8 us
  transfers between devices with their start and end apart: 9, of which 6 were waited for; matrix products, arithmetic and copies ran while one was open for 10% of the time, Pallas kernels for 0%

commit v1 on v0

--- a/solution.py
+++ b/solution.py
@@ -1,9 +1,14 @@
+import functools
+
 import jax
 import jax.numpy as jnp
 from jax import lax
+from jax.experimental import pallas as pl
+from jax.experimental.pallas import tpu as pltpu
 from jax.sharding import PartitionSpec as P
 
 norm_eps = 1e-06
+MESH = pl.DeviceIdType.MESH
 
 
 def slot_table(routes, experts, capacity):
@@ -16,17 +21,218 @@
     return flat_routes * capacity + slot_index
 
 
-def spread(gate_w, up_w, down_w):
-    gate_e, up_e, down_e = (
-        lax.all_to_all(gate_w, "tp", split_axis=0, concat_axis=2, tiled=True),
-        lax.all_to_all(up_w, "tp", split_axis=0, concat_axis=2, tiled=True),
-        lax.all_to_all(down_w, "tp", split_axis=0, concat_axis=2, tiled=True),
-    )
-    return (
-        lax.all_to_all(gate_e, "fs", split_axis=2, concat_axis=1, tiled=True),
-        lax.all_to_all(up_e, "fs", split_axis=2, concat_axis=1, tiled=True),
-        lax.all_to_all(down_e, "fs", split_axis=2, concat_axis=1, tiled=True),
-    )
+def spread_kernel(sizes, count, *refs):
+    gr, fs, tp, sub, local_experts, rows = sizes
+    ins, outs, relays = refs[:count], refs[count : 2 * count], refs[2 * count : 3 * count]
+    bounce, tp_send, tp_recv, fs_send, fs_recv, gr_send, gr_recv, load_sem, store_sem = refs[
+        3 * count :
+    ]
+    g, f, t = lax.axis_index("gr"), lax.axis_index("fs"), lax.axis_index("tp")
+    blocks = [(w, j) for j in range(local_experts) for w in range(count)]
+
+    barrier = pltpu.get_barrier_semaphore()
+    for axis, me, size in (("gr", g, gr), ("fs", f, fs), ("tp", t, tp)):
+        for d in range(1, size):
+            pl.semaphore_signal(
+                barrier, inc=1, device_id={axis: lax.rem(me + d, size)}, device_id_type=MESH
+            )
+    pl.semaphore_wait(barrier, gr + fs + tp - 3)
+
+    def out_rows(c, group, source):
+        w, j = blocks[c]
+        start = pl.multiple_of((group * fs + source) * rows, rows)
+        return outs[w].at[j, pl.ds(start, rows)]
+
+    def own(c, target, s):
+        w, j = blocks[c]
+        return ins[w].at[s, target * local_experts + j]
+
+    def relay(c, source, s):
+        w, j = blocks[c]
+        return relays[w].at[j, source, s]
+
+    def tp_copy(c, d, s, to_out):
+        target = lax.rem(t + d, tp)
+        return pltpu.make_async_remote_copy(
+            src_ref=own(c, target, s),
+            dst_ref=out_rows(c, g, f) if to_out else relay(c, t, s),
+            send_sem=tp_send.at[c, d, s],
+            recv_sem=tp_recv.at[c, d, s],
+            device_id={"tp": target},
+            device_id_type=MESH,
+        )
+
+    def fs_copy(c, d, s, src, target):
+        return pltpu.make_async_remote_copy(
+            src_ref=src,
+            dst_ref=out_rows(c, g, f),
+            send_sem=fs_send.at[c, d, s],
+            recv_sem=fs_recv.at[c, f],
+            device_id={"fs": target},
+            device_id_type=MESH,
+        )
+
+    def gr_copy(c, n, source, src):
+        return pltpu.make_async_remote_copy(
+            src_ref=src,
+            dst_ref=out_rows(c, g, source),
+            send_sem=gr_send.at[c, n, source],
+            recv_sem=gr_recv.at[c, n, source],
+            device_id={"gr": lax.rem(g + n, gr)},
+            device_id_type=MESH,
+        )
+
+    def to_groups(c, source, src):
+        for n in range(1, gr):
+            gr_copy(c, n, source, src).start()
+
+    def tp_start(c):
+        for d in range(1, tp):
+            for s in range(sub):
+
+                @pl.when(t * sub + s == f)
+                def _():
+                    tp_copy(c, d, s, True).start()
+
+                @pl.when(t * sub + s != f)
+                def _():
+                    tp_copy(c, d, s, False).start()
+
+    def own_start(c):
+        for s in range(sub):
+            target = t * sub + s
+
+            @pl.when(target != f)
+            def _():
+                fs_copy(c, 0, s, own(c, t, s), target).start()
+
+            @pl.when(target == f)
+            def _():
+                pltpu.make_async_copy(own(c, t, s), bounce.at[c], load_sem.at[c]).start()
+                to_groups(c, f, own(c, t, s))
+
+    def own_store(c):
+        for s in range(sub):
+
+            @pl.when(t * sub + s == f)
+            def _():
+                pltpu.make_async_copy(own(c, t, s), bounce.at[c], load_sem.at[c]).wait()
+                pltpu.make_async_copy(bounce.at[c], out_rows(c, g, f), store_sem.at[c]).start()
+
+    def tp_arrived(c):
+        for d in range(1, tp):
+            source = lax.rem(t + tp - d, tp)
+            for s in range(sub):
+                target = source * sub + s
+
+                @pl.when(target == f)
+                def _():
+                    tp_copy(c, d, s, True).wait_recv()
+                    to_groups(c, f, out_rows(c, g, f))
+
+                @pl.when(target != f)
+                def _():
+                    pltpu.make_async_remote_copy(
+                        src_ref=own(c, t, s),
+                        dst_ref=relay(c, source, s),
+                        send_sem=tp_send.at[c, d, s],
+                        recv_sem=tp_recv.at[c, d, s],
+                        device_id={"tp": source},
+                        device_id_type=MESH,
+                    ).wait_recv()
+                    fs_copy(c, d, s, relay(c, source, s), target).start()
+
+    def fs_arrived(c):
+        for d in range(1, fs):
+            source = lax.rem(f + d, fs)
+            pltpu.make_async_remote_copy(
+                src_ref=own(c, t, 0),
+                dst_ref=out_rows(c, g, source),
+                send_sem=fs_send.at[c, 0, 0],
+                recv_sem=fs_recv.at[c, source],
+                device_id={"fs": source},
+                device_id_type=MESH,
+            ).wait_recv()
+            to_groups(c, source, out_rows(c, g, source))
+
+    total = len(blocks)
+    ahead = min(3, total)
+    own_start(0)
+    for c in range(ahead):
+        tp_start(c)
+    for c in range(total + 1):
+        if c + ahead < total:
+            tp_start(c + ahead)
+        if c + 1 < total:
+            own_start(c + 1)
+        if c < total:
+            own_store(c)
+            tp_arrived(c)
+        if c >= 1:
+            fs_arrived(c - 1)
+
+    for c in range(total):
+        for n in range(1, gr):
+            for source in range(fs):
+                group = lax.rem(g + gr - n, gr)
+                pltpu.make_async_remote_copy(
+                    src_ref=own(c, t, 0),
+                    dst_ref=out_rows(c, group, source),
+                    send_sem=gr_send.at[c, n, source],
+                    recv_sem=gr_recv.at[c, n, source],
+                    device_id={"gr": group},
+                    device_id_type=MESH,
+                ).wait_recv()
+                gr_copy(c, n, source, out_rows(c, g, source)).wait_send()
+        for s in range(sub):
+            for d in range(1, tp):
+                tp_copy(c, d, s, False).wait_send()
+            for d in range(tp):
+                target = lax.rem(t + tp - d, tp) * sub + s
+
+                @pl.when(target != f)
+                def _():
+                    fs_copy(c, d, s, own(c, t, s), target).wait_send()
+
+            @pl.when(t * sub + s == f)
+            def _():
+                pltpu.make_async_copy(bounce.at[c], out_rows(c, g, f), store_sem.at[c]).wait()
+
+
+def spread(*weights):
+    gr, fs, tp = lax.axis_size("gr"), lax.axis_size("fs"), lax.axis_size("tp")
+    experts, rows, columns = weights[0].shape
+    local_experts = experts // tp
+    assert fs % tp == 0
+    sub = fs // tp
+    width = columns // sub
+    count = len(weights)
+    total = count * local_experts
+    parts = [w.reshape(experts, rows, sub, width).transpose(2, 0, 1, 3) for w in weights]
+    served = jax.ShapeDtypeStruct((local_experts, gr * fs * rows, width), jnp.bfloat16)
+    relayed = jax.ShapeDtypeStruct((local_experts, tp, sub, rows, width), jnp.bfloat16)
+    dma = pltpu.SemaphoreType.DMA
+    sent = 2 * total * rows * columns * (tp - 1 + fs - 1 + (gr - 1) * fs) // fs
+    found = pl.pallas_call(
+        functools.partial(spread_kernel, (gr, fs, tp, sub, local_experts, rows), count),
+        out_shape=[served] * count + [relayed] * count,
+        in_specs=[pl.BlockSpec(memory_space=pl.ANY)] * count,
+        out_specs=[pl.BlockSpec(memory_space=pl.ANY)] * (2 * count),
+        scratch_shapes=[
+            pltpu.VMEM((total, rows, width), jnp.bfloat16),
+            dma((total, tp, sub)),
+            dma((total, tp, sub)),
+            dma((total, tp, sub)),
+            dma((total, fs)),
+            dma((total, gr, fs)),
+            dma((total, gr, fs)),
+            dma((total,)),
+            dma((total,)),
+        ],
+        compiler_params=pltpu.CompilerParams(collective_id=0, has_side_effects=True),
+        cost_estimate=pl.CostEstimate(flops=0, bytes_accessed=40 * sent, transcendentals=0),
+    )(*parts)
+    return found[:count]
 
 
 def local(tokens, routes, route_weight, norm_gain, gate_master, up_master, down_master):
@@ -42,11 +248,6 @@
     up_w = (up_master * scaled_gain).astype(jnp.bfloat16)
     down_w = down_master.astype(jnp.bfloat16)
     gate_w, up_w, down_w = spread(gate_w, up_w, down_w)
-    gate_w, up_w, down_w = (
-        lax.all_gather(gate_w, "gr", axis=1, tiled=True),
-        lax.all_gather(up_w, "gr", axis=1, tiled=True),
-        lax.all_gather(down_w, "gr", axis=1, tiled=True),
-    )
     as_float = tokens.astype(jnp.float32)
     square_total = lax.psum(jnp.sum(as_float * as_float, axis=1), "fs")
     normed = (as_float * lax.rsqrt(square_total / model_width + norm_eps)[:, None]).astype(
@@ -66,10 +267,11 @@
     )
     gate_acc = jnp.einsum("sjcd,jdf->sjcf", shard_piece, gate_w, preferred_element_type=jnp.float32)
     up_acc = jnp.einsum("sjcd,jdf->sjcf", shard_piece, up_w, preferred_element_type=jnp.float32)
-    gate_acc, up_acc = (gate_acc, up_acc)
     hidden = (jax.nn.silu(gate_acc) * up_acc).astype(jnp.bfloat16)
     partial_value = jnp.einsum("sjcf,jdf->sjcd", hidden, down_w, preferred_element_type=jnp.float32)
-    summed = lax.psum_scatter(partial_value, "fs", scatter_dimension=3, tiled=True)
+    summed = lax.psum_scatter(
+        partial_value.astype(jnp.bfloat16), "fs", scatter_dimension=3, tiled=True
+    )
     produced = lax.all_to_all(summed, "tp", split_axis=0, concat_axis=0, tiled=True)
     produced = produced.reshape(experts * capacity, produced.shape[3])
     pair_slots = placing.reshape(token_rows, 2)

time: 856 us -> 604 us (0.71)
  Pallas kernels: 0 us -> 301 us
  waiting for transfers between devices: 431 us -> 145 us
  blocking collectives: 253 us -> 36.1 us
  local copies, waits for them, and re-layouts: 89.9 us -> 53.2 us
  starting transfers between devices: 15.2 us -> 4.04 us
    pallas_call x0 -> x1, Pallas kernels: none -> 301 us  [spread(): pl.pallas_call(functools.partial(spread_kernel, (gr, fs, tp, sub, local_e...]
    all_to_all x3 -> x0, blocking collectives: 217 us -> none  [the longest x1 113 us: spread(): lax.all_to_all(up_e, 'fs', split_axis=2, concat_axis=1, tiled=True)]
    all_to_all x3 -> x0, waiting for transfers between devices: 120 us -> none  [the longest x1 60.6 us: spread(): lax.all_to_all(gate_e, 'fs', split_axis=2, concat_axis=1, tiled=True)]
    reduce_scatter x1, waiting for transfers between devices: 212 us -> 145 us  [local(): lax.psum_scatter(partial_value.astype(jnp.bfloat16), 'fs', scatter_dimens...]
    all_to_all x12 -> x0, local copies, waits for them, and re-layouts: 65.4 us -> none  [the longest x2 19.2 us: spread(): lax.all_to_all(gate_w, 'tp', split_axis=0, concat_axis=2, tiled=True)]
    all_gather x3 -> x0, waiting for transfers between devices: 62.6 us -> none  [the longest x1 62.6 us: local(): lax.all_gather(down_w, 'gr', axis=1, tiled=True)]
    all_to_all x1, waiting for transfers between devices: 36.8 us -> 0.01 us  [local(): lax.all_to_all(summed, 'tp', split_axis=0, concat_axis=0, tiled=True)]
    unnamed x18 -> x15, local copies, waits for them, and re-layouts: 13.8 us -> 44.5 us
  transfers between devices with their start and end apart: 9 -> 3, of which waited for: 6 -> 1; matrix products, arithmetic and copies ran while one was open for 10% -> 9% of each run, Pallas kernels for 0% -> 50%
where the time goes in v1:
time: 604 us; the launch traced here: 602 us
  Pallas kernels  301 us (50%)
  waiting for transfers between devices  145 us (24%)
  local copies, waits for them, and re-layouts  53.2 us (9%)
  blocking collectives  36.1 us (6%)
  matrix products  32.9 us (5%)
  other arithmetic  15.9 us (3%)
  between operations  14.2 us (2%)
    pallas_call x1, Pallas kernels, spread(): pl.pallas_call(functools.partial(spread_kernel, (gr, fs, tp, sub, local_e...  301 us
    reduce_scatter x1, waiting for transfers between devices, local(): lax.psum_scatter(partial_value.astype(jnp.bfloat16), 'fs', scatter_dimens...  145 us
    unnamed x15, local copies, waits for them, and re-layouts  44.5 us
    all_to_all x1, blocking collectives, local(): lax.all_to_all(outgoing, 'tp', split_axis=0, concat_axis=0, tiled=True)  22.6 us
    psum x1, blocking collectives, local(): square_total = lax.psum(jnp.sum(as_float * as_float, axis=1), 'fs')  13.5 us
  transfers between devices with their start and end apart: 3, of which 1 were waited for; matrix products, arithmetic and copies ran while one was open for 9% of the time, Pallas kernels for 50%

profile of v1, /device:TPU:0, one launch (start us, length us, event | category | flops | bytes accessed | tf_op | source)
XLA Modules:
  0.0 602.2 jit_solution(13231430690104682705)
XLA Ops:
  7.2 0.8 copy.81
  8.0 0.2 eq.44
  8.2 0.2 eq.40
  8.4 2.3 reduce-window.6
  10.7 0.3 slice_reduce_fusion
  11.0 0.2 reduce-window.9
  11.2 0.2 reduce_sum.30
  11.5 0.7 multiply_add_fusion
  12.2 1.5 convert_reduce_fusion
  13.8 1.2 fusion.17
  15.0 13.5 %psum.7 = f32[512]{0:T(512)S(1)} all-reduce(f32[512]{0:T(512)S(1)} %fusion.17), channel_id=1, replica_groups=mesh['gr'=2,'fs'=4,'tp'=4] {'fs'}, use_global_device_ids=true, to_apply=%region_5.6 | all-reduce | flops 512 | bytes 4096 | tf_op jit(solution)/shard_map/psum | solution.py:252
  28.5 2.1 convolution_convert_fusion
  30.6 22.6 %all_to_all.10 = bf16[4,2,192,512]{3,2,1,0:T(8,128)(2,1)S(1)} all-to-all(bf16[4,2,192,512]{3,2,1,0:T(8,128)(2,1)S(1)} %bitcast.75), channel_id=1, replica_groups=mesh['gr'=2,'fs'=4,'tp'=4] {'tp'}, dimensions={0} | all-to-all | bytes 3145728 | tf_op jit(solution)/shard_map/all_to_all | solution.py:263
  53.2 1.2 copy.87
  54.5 0.2 reduce-scatter.2.cloned.1.call-start
  54.7 6.6 %copy.84 = f32[8,256,704]{2,1,0:T(8,128)} copy(f32[8,256,704]{1,2,0:T(8,128)} %param.13) | data formatting | bytes 11534336 | tf_op args[4]
  61.3 6.5 %copy.85 = f32[8,256,704]{2,1,0:T(8,128)} copy(f32[8,256,704]{1,2,0:T(8,128)} %param.14) | data formatting | bytes 11534336 | tf_op args[5]
  67.8 5.2 copy.86
  73.1 8.8 %fusion.15 = (bf16[1,8,256,704]{3,2,1,0:T(8,128)(2,1)}, bf16[1,8,256,704]{3,2,1,0:T(8,128)(2,1)}) fusion(f32[8,256,704]{2,1,0:T(8,128)} %copy.85, f32[256]{0:T(256)S(1)} %copy-done.1, f32[8,256,704]{2,1,0:T(8,128)} %copy.84), kind=kLoop, calls=%fused_computation.21 | loop fusion | flops 5767168 | bytes 17302528 | tf_op jit(solution)/shard_map/transpose;reshape | solution.py:211
  81.9 300.6 %shard_map.102 = (bf16[2,2048,704]{2,1,0:T(8,128)(2,1)}, bf16[2,2048,704]{2,1,0:T(8,128)(2,1)}, bf16[2,2048,704]{2,1,0:T(8,128)(2,1)}, bf16[2,4,1,256,704]{4,3,2...) custom-call(bf16[1,8,256,704]{3,2,1,0:T(8,128)(2,1)} %get-tuple-element.40.refs_0_, ...), custom_call_target="tpu_custom_call" | custom-call | bytes 216268800 | tf_op jit(solution)/shard_map/pallas_call | solution.py:216
  382.5 10.5 %fusion = f32[2,704,4,192]{1,3,2,0:T(8,128)} fusion(bf16[4,2,192,2048]{3,2,0,1:T(8,128)(2,1)} %all-gather.2.cloned.1.call-done, bf16[2,2048,704]{2,1,0:T(8,128)(2,1)} %get-tuple-element.33), kind=kOutput, calls=%fused_computation.2 | convolution fusion | flops 4429185024 | bytes 16384000 | tf_op jit(solution)/shard_map/sjcd,jdf->sjcf/dot_general | solution.py:269
  393.0 11.6 %fusion.6 = bf16[4,2,192,704]{3,2,0,1:T(8,128)(2,1)} fusion(f32[2,704,4,192]{1,3,2,0:T(8,128)} %fusion, bf16[4,2,192,2048]{3,2,0,1:T(8,128)(2,1)} %all-gather.2.cloned.1.call-done, bf16[2,2048,704]{2,1,0:T(8,128)(2,1)} %get-tuple-element.32), kind=kOutput, calls=%fused_computation.14 | convolution fusion | flops 4435673088 | bytes 18546688 | tf_op jit(solution)/shard_map/sjcd,jdf->sjcf/dot_general | solution.py:268
  404.6 8.7 %convert_bitcast_fusion = bf16[4,2,192,2048]{3,2,0,1:T(8,128)(2,1)} fusion(bf16[4,2,192,704]{3,2,0,1:T(8,128)(2,1)} %fusion.6, bf16[2,2048,704]{2,1,0:T(8,128)(2,1)S(1)} %bitcast.74), kind=kOutput, calls=%fused_computation.8 | convolution fusion | flops 4432330752 | bytes 14221312 | tf_op jit(solution)/shard_map/sjcf,jdf->sjcd/dot_general | solution.py:271
  413.3 145.2 %reduce-scatter.2.cloned.1.call-done = bf16[4,2,192,512]{3,2,0,1:T(8,128)(2,1)} async-done(((bf16[4,2,192,2048]{3,2,0,1:T(8,128)(2,1)}), bf16[4,2,192,512]{3,2,0,1:T(8,128)(2,1)}) %reduce-scatter.2.cloned.1.call-update) | async-done | bytes 1572880 | tf_op jit(solution)/shard_map/reduce_scatter | solution.py:272
  558.5 2.7 copy.91
  561.1 3.8 all-to-all-start.1
  564.9 8.4 %copy.92 = bf16[2,2048,704]{1,2,0:T(8,128)(2,1)} copy(bf16[2,2048,704]{2,1,0:T(8,128)(2,1)} %get-tuple-element.32) | data formatting | bytes 11534336
  573.4 8.4 %copy.93 = bf16[2,2048,704]{1,2,0:T(8,128)(2,1)} copy(bf16[2,2048,704]{2,1,0:T(8,128)(2,1)} %get-tuple-element.33) | data formatting | bytes 11534336
  581.8 8.4 %copy.94 = bf16[2,2048,704]{1,2,0:T(8,128)(2,1)} copy(bf16[2,2048,704]{2,1,0:T(8,128)(2,1)} %get-tuple-element.34) | data formatting | bytes 11534336
  590.3 2.0 gather_fusion
  592.3 2.0 gather_fusion.1
  594.2 1.1 add_convert_fusion
  (26 shorter events, 0.4 us)
Async XLA Ops:
  7.2 375.3 %all-gather.2.cloned.1.call-start = ((), (), s32[]{:S(2)}) async-start(), calls=%async_computation.3 | async-start | bytes 7864320 | tf_op jit(solution)/shard_map/all_gather | solution.py:262
  54.5 504.0 %reduce-scatter.2.cloned.1.call-start = ((), (), s32[]{:S(2)}) async-start(), calls=%async_computation.4 | async-start | bytes 7864320 | tf_op jit(solution)/shard_map/reduce_scatter | solution.py:272
  67.8 5.3 copy-start.1
  382.4 22.1 %slice-start = ((s8[6291456]{0:T(1024)(128)(4,1)}), s8[4194304]{0:T(1024)(128)(4,1)S(1)}, s32[]{:S(2)}) async-start(s8[6291456]{0:T(1024)(128)(4,1)} %bitcast.73), calls=%async_computation.5 | async-start | bytes 8388608
  393.0 11.6 %slice-start.1 = ((s8[6291456]{0:T(1024)(128)(4,1)}), s8[2097152]{0:T(1024)(128)(4,1)S(1)}, s32[]{:S(2)}) async-start(s8[6291456]{0:T(1024)(128)(4,1)} %bitcast.73), calls=%async_computation.6 | async-start | bytes 4194304
  561.1 29.1 %all-to-all-start.1 = ((bf16[4,2,192,512]{3,2,1,0:T(8,128)(2,1)}), bf16[4,2,192,512]{3,2,1,0:T(8,128)(2,1)S(1)}, u32[]{:S(2)}, u32[]{:S(2)}) async-start(bf16[4,2,192,512]{3,2,1,0:T(8,128)(2,1)} %copy.91), calls=%async_computation.2 | async-start | bytes 3145728 | tf_op jit(solution)/shard_map/all_to_all | solution.py:275
  581.8 8.5 %copy-start = (f32[512,2]{0,1:T(2,128)S(1)}, f32[512,2]{0,1:T(2,128)}, u32[]{:S(2)}) copy-start(f32[512,2]{0,1:T(2,128)} %param.11) | copy-start | bytes 12292
Sparse Core Ops, SparseCore 0:
  54.6 246.7 all-gather.1
  413.4 145.0 reduce-scatter.1

commit v2 on v1

--- a/solution.py
+++ b/solution.py
@@ -21,7 +21,7 @@
     return flat_routes * capacity + slot_index
 
 
-def spread_kernel(sizes, count, *refs):
+def spread_kernel(sizes, count, flipped, *refs):
     gr, fs, tp, sub, local_experts, rows = sizes
     ins, outs, relays = refs[:count], refs[count : 2 * count], refs[2 * count : 3 * count]
     bounce, tp_send, tp_recv, fs_send, fs_recv, gr_send, gr_recv, load_sem, store_sem = refs[
@@ -41,6 +41,8 @@
     def out_rows(c, group, source):
         w, j = blocks[c]
         start = pl.multiple_of((group * fs + source) * rows, rows)
+        if flipped:
+            return outs[w].at[j, :, pl.ds(start, rows)]
         return outs[w].at[j, pl.ds(start, rows)]
 
     def own(c, target, s):
@@ -208,18 +210,22 @@
     width = columns // sub
     count = len(weights)
     total = count * local_experts
-    parts = [w.reshape(experts, rows, sub, width).transpose(2, 0, 1, 3) for w in weights]
-    served = jax.ShapeDtypeStruct((local_experts, gr * fs * rows, width), jnp.bfloat16)
-    relayed = jax.ShapeDtypeStruct((local_experts, tp, sub, rows, width), jnp.bfloat16)
+    flipped = rows % 128 == 0
+    order = (2, 0, 3, 1) if flipped else (2, 0, 1, 3)
+    parts = [w.reshape(experts, rows, sub, width).transpose(order) for w in weights]
+    block = (width, rows) if flipped else (rows, width)
+    whole = (width, gr * fs * rows) if flipped else (gr * fs * rows, width)
+    served = jax.ShapeDtypeStruct((local_experts, *whole), jnp.bfloat16)
+    relayed = jax.ShapeDtypeStruct((local_experts, tp, sub, *block), jnp.bfloat16)
     dma = pltpu.SemaphoreType.DMA
     sent = 2 * total * rows * columns * (tp - 1 + fs - 1 + (gr - 1) * fs) // fs
     found = pl.pallas_call(
-        functools.partial(spread_kernel, (gr, fs, tp, sub, local_experts, rows), count),
+        functools.partial(spread_kernel, (gr, fs, tp, sub, local_experts, rows), count, flipped),
         out_shape=[served] * count + [relayed] * count,
         in_specs=[pl.BlockSpec(memory_space=pl.ANY)] * count,
         out_specs=[pl.BlockSpec(memory_space=pl.ANY)] * (2 * count),
         scratch_shapes=[
-            pltpu.VMEM((total, rows, width), jnp.bfloat16),
+            pltpu.VMEM((total, *block), jnp.bfloat16),
             dma((total, tp, sub)),
             dma((total, tp, sub)),
             dma((total, tp, sub)),
@@ -232,7 +238,7 @@
         compiler_params=pltpu.CompilerParams(collective_id=0, has_side_effects=True),
         cost_estimate=pl.CostEstimate(flops=0, bytes_accessed=40 * sent, transcendentals=0),
     )(*parts)
-    return found[:count]
+    return [w.swapaxes(1, 2) if flipped else w for w in found[:count]]
 
 
 def local(tokens, routes, route_weight, norm_gain, gate_master, up_master, down_master):
@@ -265,14 +271,20 @@
         axis=3,
         tiled=True,
     )
-    gate_acc = jnp.einsum("sjcd,jdf->sjcf", shard_piece, gate_w, preferred_element_type=jnp.float32)
-    up_acc = jnp.einsum("sjcd,jdf->sjcf", shard_piece, up_w, preferred_element_type=jnp.float32)
-    hidden = (jax.nn.silu(gate_acc) * up_acc).astype(jnp.bfloat16)
-    partial_value = jnp.einsum("sjcf,jdf->sjcd", hidden, down_w, preferred_element_type=jnp.float32)
-    summed = lax.psum_scatter(
-        partial_value.astype(jnp.bfloat16), "fs", scatter_dimension=3, tiled=True
-    )
-    produced = lax.all_to_all(summed, "tp", split_axis=0, concat_axis=0, tiled=True)
+    returned = []
+    for j in range(local_experts):
+        rows = shard_piece[:, j]
+        gate_acc = jnp.einsum("scd,df->scf", rows, gate_w[j], preferred_element_type=jnp.float32)
+        up_acc = jnp.einsum("scd,df->scf", rows, up_w[j], preferred_element_type=jnp.float32)
+        hidden = (jax.nn.silu(gate_acc) * up_acc).astype(jnp.bfloat16)
+        partial_value = jnp.einsum(
+            "scf,df->scd", hidden, down_w[j], preferred_element_type=jnp.float32
+        )
+        summed = lax.psum_scatter(
+            partial_value.astype(jnp.bfloat16), "fs", scatter_dimension=2, tiled=True
+        )
+        returned.append(lax.all_to_all(summed, "tp", split_axis=0, concat_axis=0, tiled=True))
+    produced = jnp.stack(returned, axis=1)
     produced = produced.reshape(experts * capacity, produced.shape[3])
     pair_slots = placing.reshape(token_rows, 2)
     first_rows = jnp.take(produced, pair_slots[:, 0], axis=0)

time: 604 us -> 574 us (0.950)
  local copies, waits for them, and re-layouts: 53.2 us -> 19.8 us
    unnamed x15 -> x18, local copies, waits for them, and re-layouts: 44.5 us -> 12.3 us
    reduce_scatter x1 -> x2, waiting for transfers between devices: 145 us -> 128 us  [local(): lax.psum_scatter(partial_value.astype(jnp.bfloat16), 'fs', scatter_dimens...]
    transpose x0 -> x2, other arithmetic: none -> 13.6 us  [spread(): w.reshape(experts, rows, sub, width).transpose(order)]
    all_to_all x1 -> x2, waiting for transfers between devices: 0.01 us -> 11.5 us  [local(): lax.all_to_all(summed, 'tp', split_axis=0, concat_axis=0, tiled=True)]
    another operation x3, other arithmetic: 11.2 us -> 2.58 us  [the longest x1 8.78 us: spread(): w.reshape(experts, rows, sub, width).transpose(2, 0, 1, 3)]
    dot_general x3 -> x4, matrix products: 30.8 us -> 37.2 us  [the longest x2 23.5 us: local(): jnp.einsum('scf,df->scd', hidden, down_w[j], preferred_element_type=jnp.f...]
  transfers between devices with their start and end apart: 3 -> 5, of which waited for: 1 -> 3; matrix products, arithmetic and copies ran while one was open for 9% -> 6% of each run, Pallas kernels for 50% -> 52%
where the time goes in v2:
time: 574 us
  Pallas kernels  297 us (52%)
  waiting for transfers between devices  140 us (24%)
  matrix products  38.2 us (7%)
  blocking collectives  36.1 us (6%)
  other arithmetic  21.2 us (4%)
  local copies, waits for them, and re-layouts  19.8 us (3%)
  between operations  13.9 us (2%)
  starting transfers between devices  7.51 us (1%)
    pallas_call x1, Pallas kernels, spread(): pl.pallas_call(functools.partial(spread_kernel, (gr, fs, tp, sub, local_e...  297 us
    reduce_scatter x2, waiting for transfers between devices, local(): lax.psum_scatter(partial_value.astype(jnp.bfloat16), 'fs', scatter_dimens...  128 us
    dot_general x2, matrix products, local(): jnp.einsum('scf,df->scd', hidden, down_w[j], preferred_element_type=jnp.f...  23.5 us
    all_to_all x1, blocking collectives, local(): lax.all_to_all(outgoing, 'tp', split_axis=0, concat_axis=0, tiled=True)  22.6 us
    dot_general x2, matrix products, local(): jnp.einsum('scd,df->scf', rows, gate_w[j], preferred_element_type=jnp.flo...  13.6 us
    transpose x2, other arithmetic, spread(): w.reshape(experts, rows, sub, width).transpose(order)  13.6 us
    psum x1, blocking collectives, local(): square_total = lax.psum(jnp.sum(as_float * as_float, axis=1), 'fs')  13.5 us
    unnamed x18, local copies, waits for them, and re-layouts  12.3 us
  transfers between devices with their start and end apart: 5, of which 3 were waited for; matrix products, arithmetic and copies ran while one was open for 6% of the time, Pallas kernels for 52%

profile of v2, /device:TPU:0, one launch (start us, length us, event | category | flops | bytes accessed | tf_op | source)
XLA Modules:
  0.0 573.9 jit_solution(8462584864646491723)
XLA Ops:
  7.2 0.9 copy.38
  8.1 0.2 eq.44
  8.5 2.3 reduce-window.6
  10.7 0.3 slice_reduce_fusion
  11.3 0.2 reduce_sum.30
  11.6 0.7 multiply_add_fusion
  12.3 1.5 convert_reduce_fusion
  13.8 0.2 fusion.9
  14.0 13.5 %psum.7 = f32[512]{0:T(512)S(1)} all-reduce(f32[512]{0:T(512)S(1)} %fusion.9), channel_id=1, replica_groups=mesh['gr'=2,'fs'=4,'tp'=4] {'fs'}, use_global_device_ids=true, to_apply=%region_5.6 | all-reduce | flops 512 | bytes 4096 | tf_op jit(solution)/shard_map/psum | solution.py:258
  27.5 1.1 convolution_convert_fusion.2
  28.6 22.6 %all_to_all.15 = bf16[4,2,192,512]{3,2,1,0:T(8,128)(2,1)S(1)} all-to-all(bf16[4,2,192,512]{3,2,1,0:T(8,128)(2,1)S(1)} %bitcast.104), channel_id=1, replica_groups=mesh['gr'=2,'fs'=4,'tp'=4] {'tp'}, dimensions={0} | all-to-all | bytes 3145728 | tf_op jit(solution)/shard_map/all_to_all | solution.py:269
  51.2 1.3 copy.41
  52.5 0.2 reduce-scatter.5.cloned.1.call-start
  52.7 4.5 convert_bitcast_fusion.refs_2_
  57.3 9.1 %fusion.1 = (bf16[1,8,704,256]{3,2,1,0:T(8,128)(2,1)}, bf16[1,8,704,256]{3,2,1,0:T(8,128)(2,1)}) fusion(f32[8,256,704]{1,2,0:T(8,128)} %param.14, f32[256]{0:T(256)S(1)} %copy-done.2, f32[8,256,704]{1,2,0:T(8,128)} %param.13), kind=kLoop, calls=%fused_computation.12 | loop fusion | flops 5767168 | bytes 17302528 | tf_op jit(solution)/shard_map/transpose | solution.py:215
  66.3 297.0 %shard_map.102 = (bf16[2,704,2048]{2,1,0:T(8,128)(2,1)}, bf16[2,704,2048]{2,1,0:T(8,128)(2,1)}, bf16[2,704,2048]{2,1,0:T(8,128)(2,1)}, bf16[2,4,1,704,256]{4,3,2...) custom-call(bf16[1,8,704,256]{3,2,1,0:T(8,128)(2,1)} %get-tuple-element.16.refs_0_, ...), custom_call_target="tpu_custom_call" | custom-call | bytes 216268800 | tf_op jit(solution)/shard_map/pallas_call | solution.py:222
  363.4 6.8 %fusion.3 = f32[4,192,704]{2,1,0:T(8,128)} fusion(bf16[2,2048,704]{1,2,0:T(8,128)(2,1)} %bitcast.99, bf16[4,2,192,2048]{3,2,0,1:T(8,128)(2,1)} %all-gather.2.cloned.1.call-done), kind=kOutput, calls=%fused_computation.17 | convolution fusion | flops 2214592512 | bytes 8192000 | tf_op jit(solution)/shard_map/scd,df->scf/dot_general | solution.py:277
  370.2 11.8 %convolution_convert_fusion = bf16[4,192,2048]{2,1,0:T(8,128)(2,1)} fusion(bf16[2,2048,704]{1,2,0:T(8,128)(2,1)} %bitcast.89, f32[4,192,704]{2,1,0:T(8,128)} %fusion.3, bf16[2,2048,704]{1,2,0:T(8,128)(2,1)} %bitcast.94, bf16[4,2,192,2048]{3,2,0,1:T(8,128)(2,1)} %all-gather.2.cloned.1.call-done), kind=kOutput, calls=%fused_computation.6 | convolution fusion | flops 4434001920 | bytes 14417920 | tf_op jit(solution)/shard_map/scf,df->scd/dot_general | solution.py:280
  382.0 0.3 reduce-scatter.3.cloned.1.call-start
  382.3 6.8 %fusion.5 = f32[4,192,704]{2,1,0:T(8,128)} fusion(bf16[2,2048,704]{1,2,0:T(8,128)(2,1)} %bitcast.100, bf16[4,2,192,2048]{3,2,0,1:T(8,128)(2,1)} %all-gather.2.cloned.1.call-done), kind=kOutput, calls=%fused_computation.22 | convolution fusion | flops 2214592512 | bytes 8192000 | tf_op jit(solution)/shard_map/scd,df->scf/dot_general | solution.py:277
  389.1 11.8 %convolution_convert_fusion.1 = bf16[4,192,2048]{2,1,0:T(8,128)(2,1)} fusion(bf16[2,2048,704]{1,2,0:T(8,128)(2,1)} %bitcast.90, f32[4,192,704]{2,1,0:T(8,128)} %fusion.5, bf16[2,2048,704]{1,2,0:T(8,128)(2,1)} %bitcast.95, bf16[4,2,192,2048]{3,2,0,1:T(8,128)(2,1)} %all-gather.2.cloned.1.call-done), kind=kOutput, calls=%fused_computation.7 | convolution fusion | flops 4434001920 | bytes 14417920 | tf_op jit(solution)/shard_map/scf,df->scd/dot_general | solution.py:280
  400.9 68.8 %reduce-scatter.5.cloned.1.call-done = bf16[4,192,512]{2,1,0:T(8,128)(2,1)} async-done(((bf16[4,192,2048]{2,1,0:T(8,128)(2,1)}), bf16[4,192,512]{2,1,0:T(8,128)(2,1)}) %reduce-scatter.5.cloned.1.call-update) | async-done | bytes 786448 | tf_op jit(solution)/shard_map/reduce_scatter | solution.py:283
  469.7 3.5 all-to-all-start.2
  473.2 59.7 %reduce-scatter.3.cloned.1.call-done = bf16[4,192,512]{2,1,0:T(8,128)(2,1)} async-done(((bf16[4,192,2048]{2,1,0:T(8,128)(2,1)}), bf16[4,192,512]{2,1,0:T(8,128)(2,1)}) %reduce-scatter.3.cloned.1.call-update) | async-done | bytes 786448 | tf_op jit(solution)/shard_map/reduce_scatter | solution.py:283
  532.9 3.5 all-to-all-start.1
  536.5 11.5 %all-to-all-done.1 = bf16[4,192,512]{2,1,0:T(8,128)(2,1)S(1)} async-done(((bf16[4,192,512]{2,1,0:T(8,128)(2,1)}), bf16[4,192,512]{2,1,0:T(8,128)(2,1)S(1)}, u32[]{:S(2)}, u32[]{:S(2)}) %all-to-all-start.1) | async-done | bytes 786464 | tf_op jit(solution)/shard_map/all_to_all | solution.py:286
  548.3 2.6 gather_fusion.1
  550.9 2.6 gather_fusion
  553.5 2.5 add_convert_fusion
  556.0 6.3 %copy.48 = bf16[2,2048,704]{1,2,0:T(8,128)(2,1)} copy(bf16[2,2048,704]{1,2,0:T(8,128)(2,1)} %bitcast.101) | data formatting | bytes 11534336
  562.3 2.5 copy.49
  564.9 2.5 copy.50
  (38 shorter events, 1.0 us)
Async XLA Ops:
  7.2 6.7 %copy-start = (bf16[512,512]{1,0:T(8,128)(2,1)S(1)}, bf16[512,512]{1,0:T(8,128)(2,1)}, u32[]{:S(2)}) copy-start(bf16[512,512]{1,0:T(8,128)(2,1)} %param.9) | copy-start | bytes 1572868
  7.2 356.2 %all-gather.2.cloned.1.call-start = ((), (), s32[]{:S(2)}) async-start(), calls=%async_computation.5 | async-start | bytes 7864320 | tf_op jit(solution)/shard_map/all_gather | solution.py:268
  52.5 4.8 copy-start.2
  52.5 417.2 %reduce-scatter.5.cloned.1.call-start = ((), (), s32[]{:S(2)}) async-start(), calls=%async_computation.7 | async-start | bytes 3932160 | tf_op jit(solution)/shard_map/reduce_scatter | solution.py:283
  382.0 150.9 %reduce-scatter.3.cloned.1.call-start = ((), (), s32[]{:S(2)}) async-start(), calls=%async_computation.6 | async-start | bytes 3932160 | tf_op jit(solution)/shard_map/reduce_scatter | solution.py:283
  400.9 135.6 %copy-start.1 = (f32[512,2]{0,1:T(2,128)S(1)}, f32[512,2]{0,1:T(2,128)}, u32[]{:S(2)}) copy-start(f32[512,2]{0,1:T(2,128)} %param.11) | copy-start | bytes 12292
  469.7 63.2 %all-to-all-start.2 = ((bf16[4,192,512]{2,1,0:T(8,128)(2,1)}), bf16[4,192,512]{2,1,0:T(8,128)(2,1)S(1)}, u32[]{:S(2)}, u32[]{:S(2)}) async-start(bf16[4,192,512]{2,1,0:T(8,128)(2,1)} %reduce-scatter.5.cloned.1.call-done), calls=%async_computation.4 | async-start | bytes 1572864 | tf_op jit(solution)/shard_map/all_to_all | solution.py:286
  532.9 15.1 %all-to-all-start.1 = ((bf16[4,192,512]{2,1,0:T(8,128)(2,1)}), bf16[4,192,512]{2,1,0:T(8,128)(2,1)S(1)}, u32[]{:S(2)}, u32[]{:S(2)}) async-start(bf16[4,192,512]{2,1,0:T(8,128)(2,1)} %reduce-scatter.3.cloned.1.call-done), calls=%async_computation.2 | async-start | bytes 1572864 | tf_op jit(solution)/shard_map/all_to_all | solution.py:286
  548.2 14.2 %slice-start.2 = ((s8[5767168]{0:T(1024)(128)(4,1)}), s8[1572864]{0:T(1024)(128)(4,1)S(1)}, s32[]{:S(2)}) async-start(s8[5767168]{0:T(1024)(128)(4,1)} %bitcast.96), calls=%async_computation.10 | async-start | bytes 3145728
  553.5 8.8 %slice-start.3 = ((s8[5767168]{0:T(1024)(128)(4,1)}), s8[4194304]{0:T(1024)(128)(4,1)S(1)}, s32[]{:S(2)}) async-start(s8[5767168]{0:T(1024)(128)(4,1)} %bitcast.96), calls=%async_computation.11 | async-start | bytes 8388608
  556.0 8.9 %slice-start = ((s8[5767168]{0:T(1024)(128)(4,1)}), s8[4194304]{0:T(1024)(128)(4,1)S(1)}, s32[]{:S(2)}) async-start(s8[5767168]{0:T(1024)(128)(4,1)} %bitcast.91), calls=%async_computation.8 | async-start | bytes 8388608
  562.3 2.5 slice-start.1
Sparse Core Ops, SparseCore 0:
  52.6 252.8 all-gather.1
  382.1 87.5 reduce-scatter.4
  472.6 60.3 reduce-scatter.2
